TPU v7x, 128 devices: a whole 4x4x4 slice. The times are simulated.
128 devices in a mesh: fs: 16 (over z, y), tp: 8 (over x, core).
Axes of the slice: x: 4, y: 4, z: 4, core: 2. Of those that a mesh axis runs over, the one named last changes fastest.
Arguments:
- late_input: bfloat16 [8192, 2048], P(('fs', 'tp')), may hold values from -6 to 6
- early_input: bfloat16 [8192, 2048], P(('fs', 'tp')), may hold values from -6 to 6
- early_grad: bfloat16 [8192, 2048], P(('fs', 'tp')), may hold values from -24 to 24
- pre_gain: float32 [2048], replicated, may hold values from 0.1 to 1.9
- post_gain: float32 [2048], replicated, may hold values from 0.1 to 1.9
- gate_weight: bfloat16 [2048, 4096], P('fs', 'tp'), may hold values from -0.125 to 0.125
- up_weight: bfloat16 [2048, 4096], P('fs', 'tp'), may hold values from -0.125 to 0.125
- down_weight: bfloat16 [2048, 4096], P('fs', 'tp'), may hold values from -0.09375 to 0.09375
- gate_sum: float32 [2048, 4096], P('fs', 'tp'), may hold values from -1.8 to 1.8
- up_sum: float32 [2048, 4096], P('fs', 'tp'), may hold values from -1.8 to 1.8
- down_gradient_sum: float32 [2048, 4096], P('fs', 'tp'), may hold values from -1.8 to 1.8
Outputs:
- late_output: bfloat16 [8192, 2048], P(('fs', 'tp'))
- early_input_grad: bfloat16 [8192, 2048], P(('fs', 'tp'))
- gate_total: float32 [2048, 4096], P('fs', 'tp')
- up_total: float32 [2048, 4096], P('fs', 'tp')
- down_total: float32 [2048, 4096], P('fs', 'tp')
All inputs are finite; a program needn't handle non-finite values.
Results may differ from a plain program's by a relative error of at most 0.013.
Values may be sent and summed in bfloat16 or wider, within the bound.
A program may use at most 128 MiB of HBM per device.

v0:
```python
import math
import jax
import jax.numpy as jnp
from jax import lax
from jax.sharding import PartitionSpec as P

NORM_EPS = 1e-06


def sent_together(arrays, axis, dim, along):
    ends, at = ([], 0)
    for a in arrays[:-1]:
        at += a.shape[along]
        ends.append(at)
    both = jnp.concatenate(arrays, axis=along)
    return tuple(jnp.split(lax.all_gather(both, axis, axis=dim, tiled=True), ends, axis=along))


def sent_to_all(shard, axis):
    peers = lax.axis_size(axis)
    return lax.all_to_all(
        jnp.broadcast_to(shard[None], (peers, *shard.shape)), axis, 0, 0, tiled=True
    )


def in_order(parts, dim):
    parts = jnp.moveaxis(parts, 0, dim)
    dims = parts.shape
    return parts.reshape(*dims[:dim], dims[dim] * dims[dim + 1], *dims[dim + 2 :])


def gather_directly(shard, axis, dim):
    parts = sent_to_all(shard, axis)
    return in_order(parts, dim)


def in_blocks(shard, dim, peers):
    dims = shard.shape
    parts = shard.reshape(*dims[:dim], peers, dims[dim] // peers, *dims[dim + 1 :])
    return jnp.moveaxis(parts, dim, 0)


def summed_on_arrival(shard, axis, dim):
    parts = in_blocks(shard, dim, lax.axis_size(axis))
    arrived = lax.all_to_all(parts, axis, split_axis=0, concat_axis=0, tiled=True)
    return arrived.astype(jnp.float32).sum(axis=0)


def contract_last(first_op, second_op):
    return lax.dot_general(
        first_op, second_op, (((1,), (1,)), ((), ())), preferred_element_type=jnp.float32
    )


def contract_first(first_op, second_op):
    return lax.dot_general(
        first_op, second_op, (((0,), (0,)), ((), ())), preferred_element_type=jnp.float32
    )


def inverse_rms(values):
    return lax.rsqrt(jnp.mean(values * values, axis=-1, keepdims=True) + NORM_EPS)


def per_device(
    late_input,
    early_input,
    early_grad,
    pre_gain,
    post_gain,
    gate_weight,
    up_weight,
    down_weight,
    gate_sum,
    up_sum,
    down_gradient_sum,
):
    tok_rows, model_width = late_input.shape
    group_rows = tok_rows * lax.axis_size("tp")
    grad_scale = 1.0 / math.sqrt(group_rows * lax.axis_size("fs"))
    hidden_width = gate_sum.shape[1]
    input_rows = jnp.stack([late_input, early_input]).astype(jnp.float32)
    input_inverse = inverse_rms(input_rows)
    normed = (input_rows * input_inverse * pre_gain).astype(jnp.bfloat16)
    normed_rows = lax.all_gather(normed, "tp", axis=1, tiled=True)
    gate_all, up_all, down_gradient_rows = sent_together(
        (gate_weight, up_weight, down_weight), "fs", 0, 1
    )
    flat_rows = normed_rows.reshape(2 * group_rows, model_width)
    gate_pre = jnp.dot(flat_rows, gate_all, preferred_element_type=jnp.float32)
    up_pre = jnp.dot(flat_rows, up_all, preferred_element_type=jnp.float32)
    hidden_state = (
        (jax.nn.silu(gate_pre) * up_pre).astype(jnp.bfloat16).reshape(2, group_rows, hidden_width)
    )
    gated_product = jnp.einsum(
        "utx,ix->tui", hidden_state, down_gradient_rows, preferred_element_type=jnp.float32
    )
    mixed_sum = lax.psum_scatter(
        gated_product.reshape(lax.axis_size("tp") * tok_rows, 2 * model_width).astype(jnp.bfloat16),
        "tp",
        scatter_dimension=0,
        tiled=True,
    ).astype(jnp.float32)
    mixed_sum = lax.optimization_barrier(mixed_sum.astype(jnp.bfloat16)).astype(jnp.float32)
    mixed_sum = mixed_sum.reshape(tok_rows, 2, model_width)
    mixed_inverse = inverse_rms(mixed_sum)
    late_output = (input_rows[0] + 0.5 * mixed_sum[:, 0] * mixed_inverse[:, 0] * post_gain).astype(
        jnp.bfloat16
    )
    early_mixed = mixed_sum[:, 1]
    early_inverse_norm = mixed_inverse[:, 1]
    weighted = 0.5 * early_grad.astype(jnp.float32) * post_gain
    mixed_cot = (
        early_inverse_norm * weighted
        - early_mixed
        * early_inverse_norm**3
        * jnp.mean(weighted * early_mixed, axis=-1, keepdims=True)
    ).astype(jnp.bfloat16)
    cot_rows = gather_directly(mixed_cot, "tp", 0)
    early_hidden = hidden_state[1]
    early_normed = normed_rows[1]
    hidden_cot = jnp.dot(cot_rows, down_gradient_rows, preferred_element_type=jnp.float32)
    early_gate = gate_pre[group_rows:]
    early_up = up_pre[group_rows:]
    sigmoid_gate = jax.nn.sigmoid(early_gate)
    gate_cot = (
        hidden_cot * early_up * sigmoid_gate * (1.0 + early_gate * (1.0 - sigmoid_gate))
    ).astype(jnp.bfloat16)
    up_cot = (hidden_cot * early_gate * sigmoid_gate).astype(jnp.bfloat16)
    normed_cot = summed_on_arrival(
        (contract_last(gate_cot, gate_all) + contract_last(up_cot, up_all)).astype(jnp.bfloat16),
        "tp",
        0,
    )
    normed_cot = lax.optimization_barrier(normed_cot.astype(jnp.bfloat16)).astype(jnp.float32)
    weighted_in = normed_cot * pre_gain
    early_values = input_rows[1]
    early_in_inverse = input_inverse[1]
    early_input_grad = (
        early_grad.astype(jnp.float32)
        + early_in_inverse * weighted_in
        - early_values
        * early_in_inverse**3
        * jnp.mean(weighted_in * early_values, axis=-1, keepdims=True)
    ).astype(jnp.bfloat16)
    totals = lax.psum_scatter(
        (
            grad_scale
            * jnp.concatenate(
                [
                    contract_first(early_normed, gate_cot),
                    contract_first(early_normed, up_cot),
                    contract_first(cot_rows, early_hidden),
                ],
                1,
            )
        ).astype(jnp.bfloat16),
        "fs",
        scatter_dimension=0,
        tiled=True,
    ).astype(jnp.float32)
    gate_total = gate_sum + totals[:, :hidden_width]
    up_total = up_sum + totals[:, hidden_width : 2 * hidden_width]
    down_total = down_gradient_sum + totals[:, 2 * hidden_width :]
    return (late_output, early_input_grad, gate_total, up_total, down_total)


def solution(mesh):
    in_specs = (
        P(("fs", "tp"), None),
        P(("fs", "tp"), None),
        P(("fs", "tp"), None),
        P(),
        P(),
        P("fs", "tp"),
        P("fs", "tp"),
        P("fs", "tp"),
        P("fs", "tp"),
        P("fs", "tp"),
        P("fs", "tp"),
    )
    out_specs = (
        P(("fs", "tp"), None),
        P(("fs", "tp"), None),
        P("fs", "tp"),
        P("fs", "tp"),
        P("fs", "tp"),
    )
    return jax.shard_map(
        per_device, mesh=mesh, in_specs=in_specs, out_specs=out_specs, check_vma=False
    )
```

profile of v0, /device:TPU:0, one launch (start us, length us, event | category | flops | bytes accessed | tf_op | source)
XLA Modules:
  0.0 314.3 jit_solution(15130578604359886631)
XLA Ops:
  7.2 1.2 multiply_reduce_fusion.1
  8.4 2.0 multiply_convert_fusion.2
  10.5 0.0 all-gather.3.cloned.1.call-start
  10.5 1.8 pad_maximum_fusion
  12.4 0.0 reduce-scatter.5.cloned.1.call-start
  12.4 32.7 %all-gather.5.cloned.1.call-done = bf16[2,512,2048]{2,1,0:T(8,128)(2,1)} async-done(((bf16[2,64,2048]{2,1,0:T(8,128)(2,1)}), bf16[2,512,2048]{2,1,0:T(8,128)(2,1)}) %all-gather.5.cloned.1.call-update) | async-done | bytes 4194320 | tf_op jit(solution)/shard_map/all_gather | solution.py:85
  45.2 63.5 %all-gather.3.cloned.1.call-done = bf16[2048,1536]{1,0:T(8,128)(2,1)} async-done(((bf16[128,1536]{1,0:T(8,128)(2,1)}), bf16[2048,1536]{1,0:T(8,128)(2,1)}) %all-gather.3.cloned.1.call-update) | async-done | bytes 6291472 | tf_op jit(solution)/shard_map/all_gather | solution.py:16
  108.7 5.3 %fusion.9 = f32[1024,512]{1,0:T(8,128)S(1)} fusion(bf16[1024,2048]{1,0:T(8,128)(2,1)} %bitcast.66, bf16[2048,1536]{1,0:T(8,128)(2,1)} %all-gather.3.cloned.1.call-done), kind=kOutput, calls=%fused_computation.14 | convolution fusion | flops 2147483648 | bytes 8388608 | tf_op jit(solution)/shard_map/dot_general | solution.py:90
  114.0 0.6 copy-done.2
  114.6 3.9 %multiply_convert_fusion = (bf16[1024,512]{1,0:T(8,128)(2,1)S(1)}, f32[1024,512]{1,0:T(8,128)}) fusion(f32[1024,512]{1,0:T(8,128)S(1)} %fusion.9, bf16[1024,2048]{1,0:T(8,128)(2,1)S(1)} %bitcast.67, bf16[2048,1536]{1,0:T(8,128)(2,1)S(1)} %copy-done.2), kind=kOutput, calls=%fused_computation.6 | convolution fusion | flops 2150629376 | bytes 11534336 | tf_op jit(solution)/shard_map/dot_general | solution.py:91
  118.5 4.4 %convolution_convert_fusion = bf16[2048,2,512]{2,0,1:T(8,128)(2,1)} fusion(bf16[2,512,512]{2,1,0:T(8,128)(2,1)S(1)} %bitcast.75, bf16[2048,1536]{1,0:T(8,128)(2,1)S(1)} %copy-done.2), kind=kOutput, calls=%fused_computation.3 | convolution fusion | flops 2149580800 | bytes 7340032 | tf_op jit(solution)/shard_map/utx,ix->tui/dot_general | solution.py:95
  122.9 6.3 %copy.39 = bf16[512,4096]{1,0:T(8,128)(2,1)} copy(bf16[512,4096]{0,1:T(8,128)(2,1)} %bitcast.68) | data formatting | bytes 8388608 | tf_op jit(solution)/shard_map/convert_element_type | solution.py:99
  129.3 0.6 copy-done.11
  129.9 36.9 %reduce-scatter.5.cloned.1.call-done = bf16[64,4096]{1,0:T(8,128)(2,1)} async-done(((bf16[512,4096]{1,0:T(8,128)(2,1)}), bf16[64,4096]{1,0:T(8,128)(2,1)}) %reduce-scatter.5.cloned.1.call-update) | async-done | bytes 524304 | tf_op jit(solution)/shard_map/reduce_scatter | solution.py:98
  166.9 2.1 reshape.128
  168.9 1.6 fusion.31
  170.6 0.5 multiply_reduce_fusion
  171.1 0.1 copy.52
  171.1 0.3 fusion.21
  171.4 0.3 fusion.20
  171.7 0.2 broadcast_in_dim.2
  172.0 29.7 %all_to_all.10 = bf16[8,64,2048]{2,1,0:T(8,128)(2,1)S(1)} all-to-all(bf16[8,64,2048]{2,1,0:T(8,128)(2,1)S(1)} %broadcast_in_dim.2), channel_id=1, replica_groups=mesh['fs'=16,'tp'=8] {'tp'}, dimensions={0} | all-to-all | bytes 4194304 | tf_op jit(solution)/shard_map/all_to_all | solution.py:21
  201.6 1.3 fusion.24
  202.9 0.3 copy-done.13
  203.2 0.6 copy-done.14
  203.8 3.3 %multiply_convert_fusion.1 = (bf16[512,512]{1,0:T(8,128)(2,1)S(1)}, bf16[512,512]{1,0:T(8,128)(2,1)S(1)}) fusion(f32[1024,512]{1,0:T(8,128)S(1)} %copy-done.13, f32[1024,512]{1,0:T(8,128)S(1)} %copy-done.14, bf16[512,2048]{1,0:T(8,128)(2,1)S(1)} %bitcast.65, bf16[2048,1536]{1,0:T(8,128)(2,1)} %all-gather.3.cloned.1.call-done), kind=kOutput, calls=%fused_computation.23 | convolution fusion | flops 1077149696 | bytes 7340032 | tf_op jit(solution)/shard_map/dot_general | solution.py:122
  207.1 1.3 fusion.2
  208.4 1.3 fusion.3
  209.8 3.8 %fusion = bf16[2048,1536]{0,1:T(8,128)(2,1)} fusion(f32[2048,512]{0,1:T(8,128)S(1)} %fusion.24, f32[2048,512]{0,1:T(8,128)S(1)} %fusion.2, f32[2048,512]{0,1:T(8,128)S(1)} %fusion.3), kind=kLoop, calls=%fused_computation.1 | loop fusion | flops 12582912 | bytes 18874368 | tf_op jit(solution)/shard_map/convert_element_type | solution.py:157
  213.6 8.6 %copy.48 = bf16[2048,1536]{1,0:T(8,128)(2,1)} copy(bf16[2048,1536]{0,1:T(8,128)(2,1)} %fusion) | data formatting | bytes 12582912
  222.3 2.9 fusion.7
  225.1 4.2 %add_convert_fusion = bf16[512,2048]{1,0:T(8,128)(2,1)} fusion(f32[512,2048]{1,0:T(8,128)S(1)} %fusion.7, bf16[512,512]{1,0:T(8,128)(2,1)S(1)} %get-tuple-element.25, bf16[2048,1536]{1,0:T(8,128)(2,1)} %all-gather.3.cloned.1.call-done), kind=kOutput, calls=%fused_computation.2 | convolution fusion | flops 1075838976 | bytes 8912896 | tf_op jit(solution)/shard_map/dot_general | solution.py:50
  229.4 3.8 %all-to-all-start.1 = ((bf16[8,64,2048]{2,1,0:T(8,128)(2,1)}), bf16[8,64,2048]{2,1,0:T(8,128)(2,1)S(1)}, u32[]{:S(2)}, u32[]{:S(2)}) async-start(bf16[8,64,2048]{2,1,0:T(8,128)(2,1)} %bitcast.14), calls=%async_computation.2 | async-start | bytes 4194304 | tf_op jit(solution)/shard_map/all_to_all | solution.py:45
  233.1 0.8 copy.44
  234.0 0.8 copy.43
  234.8 0.8 copy.42
  235.7 1.1 maximum_convert_fusion
  236.8 23.5 %all-to-all-done.1 = bf16[8,64,2048]{2,1,0:T(8,128)(2,1)S(1)} async-done(((bf16[8,64,2048]{2,1,0:T(8,128)(2,1)}), bf16[8,64,2048]{2,1,0:T(8,128)(2,1)S(1)}, u32[]{:S(2)}, u32[]{:S(2)}) %all-to-all-start.1) | async-done | bytes 2097184 | tf_op jit(solution)/shard_map/all_to_all | solution.py:45
  260.2 1.1 reduce_sum.51
  261.3 1.2 multiply_reduce_fusion.2
  262.6 2.2 fusion.23
  264.8 39.1 %reduce-scatter.7.cloned.1.call-done = bf16[128,1536]{1,0:T(8,128)(2,1)} async-done(((bf16[2048,1536]{1,0:T(8,128)(2,1)}), bf16[128,1536]{1,0:T(8,128)(2,1)}) %reduce-scatter.7.cloned.1.call-update) | async-done | bytes 393232
  303.8 1.2 copy.49
  305.1 0.1 convert_element_type.69
  305.2 0.1 slice_add_fusion
  305.2 0.8 copy.45
  306.1 0.8 copy.46
  306.9 0.8 copy.47
  (40 shorter events, 0.2 us)
Async XLA Ops:
  7.2 38.0 %all-gather.5.cloned.1.call-start = ((), (), s32[]{:S(2)}) async-start(), calls=%async_computation.5 | async-start | bytes 4718592 | tf_op jit(solution)/shard_map/all_gather | solution.py:85
  10.5 98.2 %all-gather.3.cloned.1.call-start = ((), (), s32[]{:S(2)}) async-start(), calls=%async_computation.4 | async-start | bytes 6684672 | tf_op jit(solution)/shard_map/all_gather | solution.py:16
  12.4 154.5 %reduce-scatter.5.cloned.1.call-start = ((), (), s32[]{:S(2)}) async-start(), calls=%async_computation.6 | async-start | bytes 4718592 | tf_op jit(solution)/shard_map/reduce_scatter | solution.py:98
  108.7 5.3 %copy-start = (bf16[2,512,2048]{2,1,0:T(8,128)(2,1)S(1)}, bf16[2,512,2048]{2,1,0:T(8,128)(2,1)}, u32[]{:S(2)}) copy-start(bf16[2,512,2048]{2,1,0:T(8,128)(2,1)} %all-gather.5.cloned.1.call-done) | copy-start | bytes 12582916
  108.7 5.9 %copy-start.2 = (bf16[2048,1536]{1,0:T(8,128)(2,1)S(1)}, bf16[2048,1536]{1,0:T(8,128)(2,1)}, u32[]{:S(2)}) copy-start(bf16[2048,1536]{1,0:T(8,128)(2,1)} %all-gather.3.cloned.1.call-done) | copy-start | bytes 18874372
  114.6 3.9 %copy-start.12 = (f32[1024,512]{1,0:T(8,128)}, f32[1024,512]{1,0:T(8,128)S(1)}, u32[]{:S(2)}) copy-start(f32[1024,512]{1,0:T(8,128)S(1)} %fusion.9) | copy-start | bytes 6291460
  129.2 0.7 copy-start.11
  129.2 41.9 %copy-start.3 = (bf16[64,2048]{1,0:T(8,128)(2,1)S(1)}, bf16[64,2048]{1,0:T(8,128)(2,1)}, u32[]{:S(2)}) copy-start(bf16[64,2048]{1,0:T(8,128)(2,1)} %param.13) | copy-start | bytes 786436
  129.3 174.6 %reduce-scatter.7.cloned.1.call-start = ((), (), s32[]{:S(2)}) async-start(), calls=%async_computation.7 | async-start | bytes 6684672
  201.6 1.6 copy-start.13
  201.6 2.2 copy-start.14
  203.8 3.3 %copy-start.1 = (bf16[2,512,2048]{2,1,0:T(8,128)(2,1)S(1)}, bf16[2,512,2048]{2,1,0:T(8,128)(2,1)}, u32[]{:S(2)}) copy-start(bf16[2,512,2048]{2,1,0:T(8,128)(2,1)} %all-gather.5.cloned.1.call-done) | copy-start | bytes 12582916
  229.4 3.8 %copy-start.7 = (f32[128,512]{1,0:T(8,128)S(1)}, f32[128,512]{1,0:T(8,128)}, u32[]{:S(2)}) copy-start(f32[128,512]{1,0:T(8,128)} %param.21) | copy-start | bytes 786436
  229.4 4.6 %copy-start.8 = (f32[128,512]{1,0:T(8,128)S(1)}, f32[128,512]{1,0:T(8,128)}, u32[]{:S(2)}) copy-start(f32[128,512]{1,0:T(8,128)} %param.20) | copy-start | bytes 786436
  229.4 5.5 %copy-start.9 = (f32[128,512]{1,0:T(8,128)S(1)}, f32[128,512]{1,0:T(8,128)}, u32[]{:S(2)}) copy-start(f32[128,512]{1,0:T(8,128)} %param.19) | copy-start | bytes 786436
  229.4 32.0 %copy-start.10 = (f32[2048]{0:T(1024)S(1)}, f32[2048]{0:T(1024)}, u32[]{:S(2)}) copy-start(f32[2048]{0:T(1024)} %param.14) | copy-start | bytes 24580
  229.4 30.9 %all-to-all-start.1 = ((bf16[8,64,2048]{2,1,0:T(8,128)(2,1)}), bf16[8,64,2048]{2,1,0:T(8,128)(2,1)S(1)}, u32[]{:S(2)}, u32[]{:S(2)}) async-start(bf16[8,64,2048]{2,1,0:T(8,128)(2,1)} %bitcast.14), calls=%async_computation.2 | async-start | bytes 4194304 | tf_op jit(solution)/shard_map/all_to_all | solution.py:45
  261.3 43.8 %copy-start.4 = (f32[128,512]{0,1:T(8,128)S(1)}, f32[128,512]{0,1:T(8,128)}, u32[]{:S(2)}) copy-start(f32[128,512]{0,1:T(8,128)} %copy.44) | copy-start | bytes 786436
  261.3 43.8 %copy-start.5 = (f32[128,512]{0,1:T(8,128)S(1)}, f32[128,512]{0,1:T(8,128)}, u32[]{:S(2)}) copy-start(f32[128,512]{0,1:T(8,128)} %copy.43) | copy-start | bytes 786436
  261.3 43.8 %copy-start.6 = (f32[128,512]{0,1:T(8,128)S(1)}, f32[128,512]{0,1:T(8,128)}, u32[]{:S(2)}) copy-start(f32[128,512]{0,1:T(8,128)} %copy.42) | copy-start | bytes 786436
Sparse Core Ops, SparseCore 0:
  10.6 34.4 all-gather.4
  47.3 61.3 all-gather.2
  129.4 37.4 reduce-scatter.4
  222.4 81.4 reduce-scatter.6
where the time goes:
time: 315 us; the launch traced here: 314 us
  waiting for transfers between devices  196 us (62%)
  blocking collectives  29.7 us (9%)
  matrix products  27.9 us (9%)
  local copies, waits for them, and re-layouts  27.4 us (9%)
  other arithmetic  15.7 us (5%)
  between operations  13.9 us (4%)
  starting transfers between devices  3.91 us (1%)
    all_gather x1, waiting for transfers between devices, sent_together(): lax.all_gather(both, axis, axis=dim, tiled=True)  63.5 us
    unnamed x5, waiting for transfers between devices  39.1 us
    reduce_scatter x1, waiting for transfers between devices, per_device(): lax.psum_scatter(gated_product.reshape(lax.axis_size('tp') * tok_rows, 2...  36.9 us
    all_gather x1, waiting for transfers between devices, per_device(): normed_rows = lax.all_gather(normed, 'tp', axis=1, tiled=True)  32.7 us
    all_to_all x1, blocking collectives, sent_to_all(): lax.all_to_all(jnp.broadcast_to(shard[None], (peers, *shard.shape)), axis...  29.7 us
    all_to_all x1, waiting for transfers between devices, summed_on_arrival(): lax.all_to_all(parts, axis, split_axis=0, concat_axis=0, tiled=True)  23.5 us
    unnamed x39, local copies, waits for them, and re-layouts  17.1 us
    dot_general x2, matrix products, contract_last(): lax.dot_general(first_op, second_op, (((1,), (1,)), ((), ())), preferred_...  7.09 us
  transfers between devices with their start and end apart: 5, of which 5 were waited for; matrix products, arithmetic and copies ran while one was open for 5% of the time, Pallas kernels for 0%

commit v1 on v0

--- a/solution.py
+++ b/solution.py
@@ -82,7 +82,9 @@
     input_rows = jnp.stack([late_input, early_input]).astype(jnp.float32)
     input_inverse = inverse_rms(input_rows)
     normed = (input_rows * input_inverse * pre_gain).astype(jnp.bfloat16)
-    normed_rows = lax.all_gather(normed, "tp", axis=1, tiled=True)
+    normed_rows = jnp.concatenate(
+        lax.all_to_all(jnp.stack([normed] * lax.axis_size("tp")), "tp", 0, 0), axis=1
+    )
     gate_all, up_all, down_gradient_rows = sent_together(
         (gate_weight, up_weight, down_weight), "fs", 0, 1
     )

time: 315 us -> 285 us (0.905)
  waiting for transfers between devices: 196 us -> 130 us
  blocking collectives: 29.7 us -> 53.9 us
  local copies, waits for them, and re-layouts: 27.4 us -> 32.5 us
  starting transfers between devices: 3.91 us -> 8.42 us
    all_gather x1, waiting for transfers between devices: 63.5 us -> 5.64 us  [sent_together(): lax.all_gather(both, axis, axis=dim, tiled=True)]
    all_gather x1 -> x0, waiting for transfers between devices: 32.7 us -> none  [per_device(): normed_rows = lax.all_gather(normed, 'tp', axis=1, tiled=True)]
    all_to_all x0 -> x1, waiting for transfers between devices: none -> 25.2 us  [sent_to_all(): lax.all_to_all(jnp.broadcast_to(shard[None], (peers, *shard.shape)), axis...]
    all_to_all x1, blocking collectives: 29.7 us -> 53.9 us  [per_device(): lax.all_to_all(jnp.stack([normed] * lax.axis_size('tp')), 'tp', 0, 0)]
    all_to_all x0 -> x1, starting transfers between devices: none -> 4.37 us  [sent_to_all(): lax.all_to_all(jnp.broadcast_to(shard[None], (peers, *shard.shape)), axis...]
    unnamed x5 -> x4, waiting for transfers between devices: 39.1 us -> 38.7 us
  transfers between devices with their start and end apart: 5 -> 5, of which waited for: 5 -> 5; matrix products, arithmetic and copies ran while one was open for 5% -> 8% of each run, Pallas kernels for 0% -> 0%
where the time goes in v1:
time: 285 us; the launch traced here: 284 us
  waiting for transfers between devices  130 us (46%)
  blocking collectives  53.9 us (19%)
  local copies, waits for them, and re-layouts  32.5 us (11%)
  matrix products  30.1 us (11%)
  other arithmetic  15 us (5%)
  between operations  14 us (5%)
  starting transfers between devices  8.42 us (3%)
    all_to_all x1, blocking collectives, per_device(): lax.all_to_all(jnp.stack([normed] * lax.axis_size('tp')), 'tp', 0, 0)  53.9 us
    unnamed x4, waiting for transfers between devices  38.7 us
    reduce_scatter x1, waiting for transfers between devices, per_device(): lax.psum_scatter(gated_product.reshape(lax.axis_size('tp') * tok_rows, 2...  37 us
    all_to_all x1, waiting for transfers between devices, sent_to_all(): lax.all_to_all(jnp.broadcast_to(shard[None], (peers, *shard.shape)), axis...  25.2 us
    all_to_all x1, waiting for transfers between devices, summed_on_arrival(): lax.all_to_all(parts, axis, split_axis=0, concat_axis=0, tiled=True)  23.4 us
    unnamed x39, local copies, waits for them, and re-layouts  16.3 us
    dot_general x2, matrix products, contract_last(): lax.dot_general(first_op, second_op, (((1,), (1,)), ((), ())), preferred_...  7.07 us
    convert_element_type x1, local copies, waits for them, and re-layouts, per_device(): gated_product.reshape(lax.axis_size('tp') * tok_rows, 2 * model_width)  6.37 us
  transfers between devices with their start and end apart: 5, of which 5 were waited for; matrix products, arithmetic and copies ran while one was open for 8% of the time, Pallas kernels for 0%

profile of v1, /device:TPU:0, one launch (start us, length us, event | category | flops | bytes accessed | tf_op | source)
XLA Modules:
  0.0 283.9 jit_solution(8770034890864666315)
XLA Ops:
  7.2 1.8 pad_maximum_fusion
  9.1 1.2 multiply_reduce_fusion.1
  10.4 1.2 multiply_convert_fusion.2
  11.6 0.5 stack.11
  12.1 53.9 %all_to_all.15 = bf16[8,2,64,2048]{3,2,1,0:T(8,128)(2,1)S(1)} all-to-all(bf16[8,2,64,2048]{3,2,1,0:T(8,128)(2,1)S(1)} %stack.11), channel_id=1, replica_groups=mesh['fs'=16,'tp'=8] {'tp'}, dimensions={0} | all-to-all | bytes 8388608 | tf_op jit(solution)/shard_map/all_to_all | solution.py:86
  66.0 2.3 copy.66
  68.3 5.6 %all-gather.2.cloned.1.call-done = bf16[2048,1536]{1,0:T(8,128)(2,1)} async-done(((bf16[128,1536]{1,0:T(8,128)(2,1)}), bf16[2048,1536]{1,0:T(8,128)(2,1)}) %all-gather.2.cloned.1.call-update) | async-done | bytes 6291472 | tf_op jit(solution)/shard_map/all_gather | solution.py:16
  74.0 5.3 %fusion.7 = f32[1024,512]{1,0:T(8,128)S(1)} fusion(bf16[1024,2048]{1,0:T(8,128)(2,1)} %bitcast.69, bf16[2048,1536]{1,0:T(8,128)(2,1)} %all-gather.2.cloned.1.call-done), kind=kOutput, calls=%fused_computation.11 | convolution fusion | flops 2147483648 | bytes 8388608 | tf_op jit(solution)/shard_map/dot_general | solution.py:92
  79.3 0.6 copy-done.1
  79.9 3.9 %multiply_convert_fusion = (bf16[1024,512]{1,0:T(8,128)(2,1)S(1)}, f32[1024,512]{1,0:T(8,128)}) fusion(f32[1024,512]{1,0:T(8,128)S(1)} %fusion.7, bf16[1024,2048]{1,0:T(8,128)(2,1)S(1)} %bitcast.71, bf16[2048,1536]{1,0:T(8,128)(2,1)S(1)} %copy-done.1), kind=kOutput, calls=%fused_computation.5 | convolution fusion | flops 2150629376 | bytes 11534336 | tf_op jit(solution)/shard_map/dot_general | solution.py:93
  83.8 4.4 %convolution_convert_fusion = bf16[2048,2,512]{2,0,1:T(8,128)(2,1)} fusion(bf16[2,512,512]{2,1,0:T(8,128)(2,1)S(1)} %bitcast.79, bf16[2048,1536]{1,0:T(8,128)(2,1)S(1)} %copy-done.1), kind=kOutput, calls=%fused_computation.3 | convolution fusion | flops 2149580800 | bytes 7340032 | tf_op jit(solution)/shard_map/utx,ix->tui/dot_general | solution.py:97
  88.2 6.4 %copy.41 = bf16[512,4096]{1,0:T(8,128)(2,1)} copy(bf16[512,4096]{0,1:T(8,128)(2,1)} %bitcast.72) | data formatting | bytes 8388608 | tf_op jit(solution)/shard_map/convert_element_type | solution.py:101
  94.6 0.7 copy-done.11
  95.3 37.0 %reduce-scatter.5.cloned.1.call-done = bf16[64,4096]{1,0:T(8,128)(2,1)} async-done(((bf16[512,4096]{1,0:T(8,128)(2,1)}), bf16[64,4096]{1,0:T(8,128)(2,1)}) %reduce-scatter.5.cloned.1.call-update) | async-done | bytes 524304 | tf_op jit(solution)/shard_map/reduce_scatter | solution.py:100
  132.3 2.1 reshape.140
  134.3 1.6 fusion.29
  135.9 0.5 multiply_reduce_fusion
  136.4 0.1 copy.54
  136.5 0.3 fusion.19
  136.8 0.3 fusion.18
  137.1 1.6 broadcast_in_dim.2
  138.7 4.4 %all-to-all-start.1 = ((bf16[8,64,2048]{2,1,0:T(8,128)(2,1)}), bf16[8,64,2048]{2,1,0:T(8,128)(2,1)}, u32[]{:S(2)}, u32[]{:S(2)}) async-start(bf16[8,64,2048]{2,1,0:T(8,128)(2,1)} %broadcast_in_dim.2), calls=%async_computation.2 | async-start | bytes 4194304 | tf_op jit(solution)/shard_map/all_to_all | solution.py:21
  143.0 0.2 reduce-scatter.7.cloned.1.call-start
  143.3 1.7 slice.65
  145.0 25.2 %all-to-all-done.1 = bf16[8,64,2048]{2,1,0:T(8,128)(2,1)} async-done(((bf16[8,64,2048]{2,1,0:T(8,128)(2,1)}), bf16[8,64,2048]{2,1,0:T(8,128)(2,1)}, u32[]{:S(2)}, u32[]{:S(2)}) %all-to-all-start.1) | async-done | bytes 2097184 | tf_op jit(solution)/shard_map/all_to_all | solution.py:21
  170.2 3.1 %fusion.22 = f32[2048,512]{0,1:T(8,128)S(1)} fusion(bf16[512,2048]{1,0:T(8,128)(2,1)} %bitcast.15, bf16[1024,512]{1,0:T(8,128)(2,1)} %copy-done.6), kind=kOutput, calls=%fused_computation.34 | convolution fusion | flops 1073741824 | bytes 6815744 | tf_op jit(solution)/shard_map/dot_general | solution.py:56
  173.4 3.8 %multiply_convert_fusion.1 = (bf16[512,512]{1,0:T(8,128)(2,1)S(1)}, bf16[512,512]{1,0:T(8,128)(2,1)S(1)}) fusion(f32[1024,512]{1,0:T(8,128)S(1)} %copy-done.13, f32[1024,512]{1,0:T(8,128)S(1)} %copy-done.14, bf16[512,2048]{1,0:T(8,128)(2,1)} %bitcast.15, bf16[2048,1536]{1,0:T(8,128)(2,1)} %all-gather.2.cloned.1.call-done), kind=kOutput, calls=%fused_computation.20 | convolution fusion | flops 1077149696 | bytes 7340032 | tf_op jit(solution)/shard_map/dot_general | solution.py:124
  177.1 1.3 fusion.31
  178.4 1.3 fusion.30
  179.8 3.9 %fusion = bf16[2048,1536]{0,1:T(8,128)(2,1)} fusion(f32[2048,512]{0,1:T(8,128)S(1)} %fusion.22, f32[2048,512]{0,1:T(8,128)S(1)} %fusion.31, f32[2048,512]{0,1:T(8,128)S(1)} %fusion.30), kind=kLoop, calls=%fused_computation.1 | loop fusion | flops 12582912 | bytes 18874368 | tf_op jit(solution)/shard_map/convert_element_type | solution.py:159
  183.6 8.7 %copy.50 = bf16[2048,1536]{1,0:T(8,128)(2,1)} copy(bf16[2048,1536]{0,1:T(8,128)(2,1)} %fusion) | data formatting | bytes 12582912
  192.3 2.9 %fusion.5 = f32[512,2048]{1,0:T(8,128)S(1)} fusion(bf16[512,512]{1,0:T(8,128)(2,1)S(1)} %get-tuple-element.28, bf16[2048,1536]{1,0:T(8,128)(2,1)} %all-gather.2.cloned.1.call-done), kind=kOutput, calls=%fused_computation.9 | convolution fusion | flops 1073741824 | bytes 6815744 | tf_op jit(solution)/shard_map/dot_general | solution.py:50
  195.2 4.2 %add_convert_fusion = bf16[512,2048]{1,0:T(8,128)(2,1)} fusion(f32[512,2048]{1,0:T(8,128)S(1)} %fusion.5, bf16[512,512]{1,0:T(8,128)(2,1)S(1)} %get-tuple-element.27, bf16[2048,1536]{1,0:T(8,128)(2,1)} %all-gather.2.cloned.1.call-done), kind=kOutput, calls=%fused_computation.2 | convolution fusion | flops 1075838976 | bytes 8912896 | tf_op jit(solution)/shard_map/dot_general | solution.py:50
  199.4 3.8 %all-to-all-start.2 = ((bf16[8,64,2048]{2,1,0:T(8,128)(2,1)}), bf16[8,64,2048]{2,1,0:T(8,128)(2,1)S(1)}, u32[]{:S(2)}, u32[]{:S(2)}) async-start(bf16[8,64,2048]{2,1,0:T(8,128)(2,1)} %bitcast.16), calls=%async_computation.3 | async-start | bytes 4194304 | tf_op jit(solution)/shard_map/all_to_all | solution.py:45
  203.2 0.8 copy.46
  204.0 0.8 copy.45
  204.8 0.8 copy.44
  205.7 1.1 maximum_convert_fusion
  206.8 23.4 %all-to-all-done.2 = bf16[8,64,2048]{2,1,0:T(8,128)(2,1)S(1)} async-done(((bf16[8,64,2048]{2,1,0:T(8,128)(2,1)}), bf16[8,64,2048]{2,1,0:T(8,128)(2,1)S(1)}, u32[]{:S(2)}, u32[]{:S(2)}) %all-to-all-start.2) | async-done | bytes 2097184 | tf_op jit(solution)/shard_map/all_to_all | solution.py:45
  230.2 1.1 reduce_sum.51
  231.4 1.2 multiply_reduce_fusion.2
  232.6 2.2 fusion.21
  234.8 38.7 %reduce-scatter.7.cloned.1.call-done = bf16[128,1536]{1,0:T(8,128)(2,1)} async-done(((bf16[2048,1536]{1,0:T(8,128)(2,1)}), bf16[128,1536]{1,0:T(8,128)(2,1)}) %reduce-scatter.7.cloned.1.call-update) | async-done | bytes 393232
  273.5 1.2 copy.51
  274.8 0.1 slice_add_fusion
  274.9 0.8 copy.47
  275.7 0.8 copy.48
  276.6 0.8 copy.49
  (42 shorter events, 0.3 us)
Async XLA Ops:
  7.2 66.8 %all-gather.2.cloned.1.call-start = ((), (), s32[]{:S(2)}) async-start(), calls=%async_computation.5 | async-start | bytes 6684672 | tf_op jit(solution)/shard_map/all_gather | solution.py:16
  9.1 123.2 %reduce-scatter.5.cloned.1.call-start = ((), (), s32[]{:S(2)}) async-start(), calls=%async_computation.6 | async-start | bytes 4718592 | tf_op jit(solution)/shard_map/reduce_scatter | solution.py:100
  74.0 5.3 %copy-start = (bf16[8,2,64,2048]{3,2,0,1:T(8,128)(2,1)S(1)}, bf16[8,2,64,2048]{3,2,0,1:T(8,128)(2,1)}, u32[]{:S(2)}) copy-start(bf16[8,2,64,2048]{3,2,0,1:T(8,128)(2,1)} %copy.66) | copy-start | bytes 12582916
  74.0 5.9 %copy-start.1 = (bf16[2048,1536]{1,0:T(8,128)(2,1)S(1)}, bf16[2048,1536]{1,0:T(8,128)(2,1)}, u32[]{:S(2)}) copy-start(bf16[2048,1536]{1,0:T(8,128)(2,1)} %all-gather.2.cloned.1.call-done) | copy-start | bytes 18874372
  79.9 3.9 %copy-start.12 = (f32[1024,512]{1,0:T(8,128)}, f32[1024,512]{1,0:T(8,128)S(1)}, u32[]{:S(2)}) copy-start(f32[1024,512]{1,0:T(8,128)S(1)} %fusion.7) | copy-start | bytes 6291460
  83.8 4.4 %copy-start.6 = (bf16[1024,512]{1,0:T(8,128)(2,1)}, bf16[1024,512]{1,0:T(8,128)(2,1)S(1)}, u32[]{:S(2)}) copy-start(bf16[1024,512]{1,0:T(8,128)(2,1)S(1)} %get-tuple-element.38) | copy-start | bytes 3145732
  94.6 0.7 copy-start.11
  94.6 41.9 %copy-start.2 = (bf16[64,2048]{1,0:T(8,128)(2,1)S(1)}, bf16[64,2048]{1,0:T(8,128)(2,1)}, u32[]{:S(2)}) copy-start(bf16[64,2048]{1,0:T(8,128)(2,1)} %param.13) | copy-start | bytes 786436
  138.7 31.5 %all-to-all-start.1 = ((bf16[8,64,2048]{2,1,0:T(8,128)(2,1)}), bf16[8,64,2048]{2,1,0:T(8,128)(2,1)}, u32[]{:S(2)}, u32[]{:S(2)}) async-start(bf16[8,64,2048]{2,1,0:T(8,128)(2,1)} %broadcast_in_dim.2), calls=%async_computation.2 | async-start | bytes 4194304 | tf_op jit(solution)/shard_map/all_to_all | solution.py:21
  143.0 130.4 %reduce-scatter.7.cloned.1.call-start = ((), (), s32[]{:S(2)}) async-start(), calls=%async_computation.7 | async-start | bytes 6684672
  170.2 3.1 %copy-start.13 = (f32[1024,512]{1,0:T(8,128)S(1)}, f32[1024,512]{1,0:T(8,128)}, u32[]{:S(2)}) copy-start(f32[1024,512]{1,0:T(8,128)} %copy-done.12) | copy-start | bytes 6291460
  170.2 3.1 %copy-start.14 = (f32[1024,512]{1,0:T(8,128)S(1)}, f32[1024,512]{1,0:T(8,128)}, u32[]{:S(2)}) copy-start(f32[1024,512]{1,0:T(8,128)} %get-tuple-element.39) | copy-start | bytes 6291460
  199.4 3.8 %copy-start.7 = (f32[128,512]{1,0:T(8,128)S(1)}, f32[128,512]{1,0:T(8,128)}, u32[]{:S(2)}) copy-start(f32[128,512]{1,0:T(8,128)} %param.21) | copy-start | bytes 786436
  199.4 4.6 %copy-start.8 = (f32[128,512]{1,0:T(8,128)S(1)}, f32[128,512]{1,0:T(8,128)}, u32[]{:S(2)}) copy-start(f32[128,512]{1,0:T(8,128)} %param.20) | copy-start | bytes 786436
  199.4 5.5 %copy-start.9 = (f32[128,512]{1,0:T(8,128)S(1)}, f32[128,512]{1,0:T(8,128)}, u32[]{:S(2)}) copy-start(f32[128,512]{1,0:T(8,128)} %param.19) | copy-start | bytes 786436
  199.4 32.0 %copy-start.10 = (f32[2048]{0:T(1024)S(1)}, f32[2048]{0:T(1024)}, u32[]{:S(2)}) copy-start(f32[2048]{0:T(1024)} %param.14) | copy-start | bytes 24580
  199.4 30.9 %all-to-all-start.2 = ((bf16[8,64,2048]{2,1,0:T(8,128)(2,1)}), bf16[8,64,2048]{2,1,0:T(8,128)(2,1)S(1)}, u32[]{:S(2)}, u32[]{:S(2)}) async-start(bf16[8,64,2048]{2,1,0:T(8,128)(2,1)} %bitcast.16), calls=%async_computation.3 | async-start | bytes 4194304 | tf_op jit(solution)/shard_map/all_to_all | solution.py:45
  231.3 43.4 %copy-start.3 = (f32[128,512]{0,1:T(8,128)S(1)}, f32[128,512]{0,1:T(8,128)}, u32[]{:S(2)}) copy-start(f32[128,512]{0,1:T(8,128)} %copy.46) | copy-start | bytes 786436
  231.3 43.4 %copy-start.4 = (f32[128,512]{0,1:T(8,128)S(1)}, f32[128,512]{0,1:T(8,128)}, u32[]{:S(2)}) copy-start(f32[128,512]{0,1:T(8,128)} %copy.45) | copy-start | bytes 786436
  231.4 43.4 %copy-start.5 = (f32[128,512]{0,1:T(8,128)S(1)}, f32[128,512]{0,1:T(8,128)}, u32[]{:S(2)}) copy-start(f32[128,512]{0,1:T(8,128)} %copy.44) | copy-start | bytes 786436
Sparse Core Ops, SparseCore 0:
  10.1 63.8 all-gather.1
  94.7 37.4 reduce-scatter.4
  192.4 81.0 reduce-scatter.6
